TPU v7x, 32 devices: a whole 2x2x4 slice. The times are simulated.
32 devices in a mesh: sp: 8 (over z, x), tp: 4 (over y, core).
Axes of the slice: x: 2, y: 2, z: 4, core: 2. Of those that a mesh axis runs over, the one named last changes fastest.
Arguments:
- cotangent: bfloat16 [1024, 2048], P('sp'), may hold values from -6 to 6
- mixer_out: bfloat16 [1024, 2048], P('sp'), may hold values from -6 to 6
- expert_ids: int32 [1024, 2], P('sp'), may hold values from 0 to 7, all different within a row; in each aligned block of 128 rows (0 to 127, 128 to 255, ...) at most 64 rows name the same one
- route_weight: float32 [1024, 2], P('sp'), may hold values from 0.3 to 1.5
- saved_normalized: bfloat16 [1024, 2048], P('sp', 'tp'), may hold values from -6 to 6
- inverse_deviation: float32 [1024], P('sp'), may hold values from 0.3 to 3
- channel_norm_gain: float32 [2048], P('tp'), may hold values from 0.1 to 1.9
- taps: float32 [31, 2048], P(None, 'tp'), may hold values from -1 to 1
- proj_weight: bfloat16 [2048, 2048], P('tp'), may hold values from -0.125 to 0.125
- gate_weight: bfloat16 [8, 2048, 2048], P('sp', None, 'tp'), may hold values from -0.125 to 0.125
- up_weight: bfloat16 [8, 2048, 2048], P('sp', None, 'tp'), may hold values from -0.125 to 0.125
- down_weight: bfloat16 [8, 2048, 2048], P('sp', 'tp'), may hold values from -0.125 to 0.125
Outputs:
- grad_mixer_in: bfloat16 [1024, 2048], P('sp', 'tp')
- grad_proj: float32 [2048, 2048], P('sp', 'tp')
- grad_gate: bfloat16 [8, 2048, 2048], P('sp', None, 'tp')
- grad_up: bfloat16 [8, 2048, 2048], P('sp', None, 'tp')
- grad_down: bfloat16 [8, 2048, 2048], P('sp', 'tp')
Inputs may be any that keep to these rules, and one draw needn't show every extreme that they name: `expert_ids`: each row names 2 different experts. Within the rows of one index of sp no expert is named more than 64 times, a bound that some block reaches.
All inputs are finite; a program needn't handle non-finite values.
Results may differ from a plain program's by a relative error of at most 0.02.
Values may be sent and summed in bfloat16 or wider, within the bound.
A program may use at most 64 MiB of HBM per device.

v0:
```python
import jax
import jax.numpy as jnp
from jax import lax
from jax.sharding import PartitionSpec as P


def from_behind(value, axis, steps):
    count = lax.axis_size(axis)
    leading, last = (max(0, -steps), min(count, count - steps))
    return lax.ppermute(value, axis, [(source, source + steps) for source in range(leading, last)])


def route_table(expert_ids, route_weight, slot_start, slot_span, capacity, experts):
    onehot = (expert_ids[:, :, None] == jnp.arange(experts, dtype=jnp.int32)[None, None, :]).astype(
        jnp.int32
    )
    flat_hot = onehot.reshape(-1, experts)
    ranks = jnp.cumsum(flat_hot, axis=0) - flat_hot
    rank_pair = jnp.sum(ranks * flat_hot, axis=1).reshape(expert_ids.shape)
    slot_index = expert_ids * capacity + rank_pair
    targets = (
        jnp.arange(experts, dtype=jnp.int32)[:, None] * capacity
        + slot_start
        + jnp.arange(slot_span, dtype=jnp.int32)[None, :]
    ).reshape(-1)
    matched = slot_index[None, :, :] == targets[:, None, None]
    dispatch = jnp.any(matched, axis=2).astype(jnp.bfloat16)
    slot_weight = jnp.sum(jnp.where(matched, route_weight[None, :, :], 0.0), axis=(1, 2))
    return (dispatch, slot_weight)


def shards(
    cotangent,
    mixer_out,
    expert_ids,
    route_weight,
    saved_normalized,
    inverse_deviation,
    channel_norm_gain,
    taps,
    proj_weight,
    gate_weight,
    up_weight,
    down_weight,
):
    experts = lax.axis_size("sp")
    groups = lax.axis_size("tp")
    tok_rows, model_width = cotangent.shape
    capacity = groups * max(1, 4 * tok_rows // (experts * groups))
    slot_span = capacity // groups
    slot_start = lax.axis_index("tp") * slot_span
    dispatch, slot_weight = route_table(
        expert_ids, route_weight, slot_start, slot_span, capacity, experts
    )
    sent_rows = jnp.dot(dispatch, mixer_out, preferred_element_type=jnp.float32).astype(
        jnp.bfloat16
    )
    sent_grad = (
        slot_weight[:, None] * jnp.dot(dispatch, cotangent, preferred_element_type=jnp.float32)
    ).astype(jnp.bfloat16)
    sent_rows = sent_rows.reshape(experts, slot_span, model_width)
    sent_grad = sent_grad.reshape(experts, slot_span, model_width)
    shared_rows = (
        lax.all_to_all(sent_rows, "sp", split_axis=0, concat_axis=0, tiled=True),
        lax.all_to_all(sent_grad, "sp", split_axis=0, concat_axis=0, tiled=True),
    )
    routed_rows, routed_grad = (
        lax.all_gather(shared_rows[0], "tp", axis=1, tiled=True),
        lax.all_gather(shared_rows[1], "tp", axis=1, tiled=True),
    )
    full_table, unused_weight = route_table(
        expert_ids, route_weight, 0, capacity, capacity, experts
    )
    routed_rows = routed_rows.reshape(-1, model_width)
    routed_grad = routed_grad.reshape(-1, model_width)
    w_first = gate_weight[0]
    w_third = up_weight[0]
    w_second = down_weight[0]
    contract_last = (((1,), (1,)), ((), ()))
    contract_first = (((0,), (0,)), ((), ()))
    hidden_gate = jnp.dot(routed_rows, w_first, preferred_element_type=jnp.float32)
    hidden_up = jnp.dot(routed_rows, w_third, preferred_element_type=jnp.float32)
    sigma = jax.nn.sigmoid(hidden_gate)
    swish = hidden_gate * sigma
    activ = (swish * hidden_up).astype(jnp.bfloat16)
    grad_second = lax.dot_general(
        activ, routed_grad, contract_first, preferred_element_type=jnp.float32
    ).astype(jnp.bfloat16)
    grad_activ = lax.dot_general(
        routed_grad, w_second, contract_last, preferred_element_type=jnp.float32
    )
    grad_gpre = (grad_activ * hidden_up * sigma * (1.0 + hidden_gate * (1.0 - sigma))).astype(
        jnp.bfloat16
    )
    grad_upre = (grad_activ * swish).astype(jnp.bfloat16)
    grad_first = lax.dot_general(
        routed_rows, grad_gpre, contract_first, preferred_element_type=jnp.float32
    ).astype(jnp.bfloat16)
    grad_third = lax.dot_general(
        routed_rows, grad_upre, contract_first, preferred_element_type=jnp.float32
    ).astype(jnp.bfloat16)
    partial_value = lax.dot_general(
        grad_gpre, w_first, contract_last, preferred_element_type=jnp.float32
    ) + lax.dot_general(grad_upre, w_third, contract_last, preferred_element_type=jnp.float32)
    summed = lax.psum(partial_value.astype(jnp.bfloat16), "tp")
    home_rows = lax.all_to_all(
        summed.reshape(experts, capacity, model_width),
        "sp",
        split_axis=0,
        concat_axis=0,
        tiled=True,
    )
    returned = lax.dot_general(
        full_table,
        home_rows.reshape(-1, model_width),
        contract_first,
        preferred_element_type=jnp.float32,
    )
    mixer_grad = (cotangent.astype(jnp.float32) + returned).astype(jnp.bfloat16)
    normalized_input = saved_normalized.astype(jnp.float32)
    normalized_values = normalized_input * channel_norm_gain[None, :]
    gate_sig = jax.nn.sigmoid(normalized_values)
    act_conv = (normalized_values * gate_sig).astype(jnp.bfloat16)
    grad_proj = lax.psum_scatter(
        lax.dot_general(
            mixer_grad, act_conv, contract_first, preferred_element_type=jnp.float32
        ).astype(jnp.bfloat16),
        "sp",
        scatter_dimension=0,
        tiled=True,
    ).astype(jnp.float32)
    grad_act = lax.dot_general(
        mixer_grad, proj_weight, contract_last, preferred_element_type=jnp.float32
    )
    norm_output_gradient = (
        grad_act
        * gate_sig
        * (1.0 + normalized_values * (1.0 - gate_sig))
        * channel_norm_gain[None, :]
    )
    reduced_totals = lax.psum(
        (
            jnp.sum(norm_output_gradient, axis=1),
            jnp.sum(norm_output_gradient * normalized_input, axis=1),
        ),
        "tp",
    )
    channel_count = saved_normalized.shape[1] * groups
    conv_output_gradient = inverse_deviation[:, None] * (
        norm_output_gradient
        - reduced_totals[0][:, None] / channel_count
        - normalized_input * (reduced_totals[1][:, None] / channel_count)
    )
    reach = taps.shape[0] - 1
    beyond = from_behind(conv_output_gradient[:reach], "sp", -1)
    extended = jnp.concatenate([conv_output_gradient, beyond], axis=0)
    result = jnp.zeros_like(conv_output_gradient)
    for tap_index in range(taps.shape[0]):
        result = result + taps[tap_index][None, :] * extended[tap_index : tap_index + tok_rows]
    return (
        result.astype(jnp.bfloat16),
        grad_proj,
        grad_first[None],
        grad_third[None],
        grad_second[None],
    )


def solution(mesh):
    return jax.shard_map(
        shards,
        mesh=mesh,
        in_specs=(
            P("sp", None),
            P("sp", None),
            P("sp", None),
            P("sp", None),
            P("sp", "tp"),
            P("sp"),
            P("tp"),
            P(None, "tp"),
            P("tp", None),
            P("sp", None, "tp"),
            P("sp", None, "tp"),
            P("sp", "tp", None),
        ),
        out_specs=(
            P("sp", "tp"),
            P("sp", "tp"),
            P("sp", None, "tp"),
            P("sp", None, "tp"),
            P("sp", "tp", None),
        ),
        check_vma=False,
    )
```

profile of v0, /device:TPU:0, one launch (start us, length us, event | category | flops | bytes accessed | tf_op | source)
XLA Modules:
  0.0 273.1 jit_solution(8081440627756328696)
XLA Ops:
  10.6 1.3 convolution_convert_fusion.4
  11.9 21.7 %all_to_all.15 = bf16[8,16,2048]{2,1,0:T(8,128)(2,1)} all-to-all(bf16[8,16,2048]{2,1,0:T(8,128)(2,1)S(1)} %bitcast.87), channel_id=1, replica_groups=mesh['sp'=8,'tp'=4] {'sp'}, dimensions={0} | all-to-all | bytes 1048576 | tf_op jit(solution)/shard_map/all_to_all | solution.py:64
  34.2 17.6 %all_to_all.16 = bf16[8,16,2048]{2,1,0:T(8,128)(2,1)} all-to-all(bf16[8,16,2048]{2,1,0:T(8,128)(2,1)S(1)} %bitcast.86), channel_id=1, replica_groups=mesh['sp'=8,'tp'=4] {'sp'}, dimensions={0} | all-to-all | bytes 1048576 | tf_op jit(solution)/shard_map/all_to_all | solution.py:65
  51.9 3.5 %all-gather.5.cloned.1.call-done = bf16[8,64,2048]{2,1,0:T(8,128)(2,1)} async-done(((bf16[8,16,2048]{2,1,0:T(8,128)(2,1)}), bf16[8,64,2048]{2,1,0:T(8,128)(2,1)}) %all-gather.5.cloned.1.call-update) | async-done | bytes 2097168 | tf_op jit(solution)/shard_map/all_gather | solution.py:68
  55.4 4.0 %fusion.7 = f32[512,512]{1,0:T(8,128)} fusion(bf16[512,2048]{1,0:T(8,128)(2,1)} %bitcast.119, bf16[1,2048,512]{2,1,0:T(8,128)(2,1)S(1)} %copy-done), kind=kOutput, calls=%fused_computation.44 | convolution fusion | flops 1073741824 | bytes 5242880 | tf_op jit(solution)/shard_map/dot_general | solution.py:81
  59.4 2.3 fusion.10
  61.7 17.9 %all-gather.3.cloned.1.call-done = bf16[8,64,2048]{2,1,0:T(8,128)(2,1)} async-done(((bf16[8,16,2048]{2,1,0:T(8,128)(2,1)}), bf16[8,64,2048]{2,1,0:T(8,128)(2,1)}) %all-gather.3.cloned.1.call-update) | async-done | bytes 2097168 | tf_op jit(solution)/shard_map/all_gather | solution.py:69
  79.6 4.4 %multiply_convert_fusion.1 = (bf16[512,512]{1,0:T(8,128)(2,1)S(1)}, bf16[512,512]{1,0:T(8,128)(2,1)S(1)}) fusion(f32[512,512]{1,0:T(8,128)} %fusion.7, f32[512,512]{1,0:T(8,128)} %fusion.10, bf16[512,2048]{1,0:T(8,128)(2,1)} %bitcast.123, bf16[1,512,2048]{2,1,0:T(8,128)(2,1)} %param.23), kind=kOutput, calls=%fused_computation.55 | convolution fusion | flops 1077149696 | bytes 7340032 | tf_op jit(solution)/shard_map/dot_general | solution.py:89
  84.0 1.3 fusion.5
  85.9 2.6 add_convert_fusion
  88.6 51.5 %all-reduce.3.cloned.1.call-done = bf16[8,64,2048]{2,1,0:T(8,128)(2,1)} async-done(((bf16[8,64,2048]{2,1,0:T(8,128)(2,1)}), bf16[8,64,2048]{2,1,0:T(8,128)(2,1)}) %all-reduce.3.cloned.1.call-update) | async-done | bytes 2097168 | tf_op jit(solution)/shard_map/psum | solution.py:105
  140.1 5.5 %all-to-all-start.2 = ((bf16[8,64,2048]{2,1,0:T(8,128)(2,1)}), bf16[8,64,2048]{2,1,0:T(8,128)(2,1)}, u32[]{:S(2)}, u32[]{:S(2)}) async-start(bf16[8,64,2048]{2,1,0:T(8,128)(2,1)} %all-reduce.3.cloned.1.call-done), calls=%async_computation.2 | async-start | bytes 4194304 | tf_op jit(solution)/shard_map/all_to_all | solution.py:106
  146.0 47.7 %all-to-all-done.2 = bf16[8,64,2048]{2,1,0:T(8,128)(2,1)} async-done(((bf16[8,64,2048]{2,1,0:T(8,128)(2,1)}), bf16[8,64,2048]{2,1,0:T(8,128)(2,1)}, u32[]{:S(2)}, u32[]{:S(2)}) %all-to-all-start.2) | async-done | bytes 2097184 | tf_op jit(solution)/shard_map/all_to_all | solution.py:106
  193.7 2.1 fusion.4
  195.8 2.1 convolution_convert_fusion
  199.3 4.4 %fusion.1 = bf16[1,2048,512]{2,1,0:T(8,128)(2,1)} fusion(bf16[512,2048]{1,0:T(8,128)(2,1)} %bitcast.120, bf16[512,512]{1,0:T(8,128)(2,1)S(1)} %copy-done.7), kind=kOutput, calls=%fused_computation.35 | convolution fusion | flops 1074790400 | bytes 4718592 | tf_op jit(solution)/shard_map/dot_general | solution.py:99
  203.7 2.7 fusion.2
  206.4 1.5 fusion.128
  207.9 6.2 %all-reduce = (f32[128]{0:T(128)S(1)}, f32[128]{0:T(128)S(1)}) all-reduce(f32[128]{0:T(128)} %get-tuple-element.6, f32[128]{0:T(128)} %get-tuple-element.5), channel_id=1, replica_groups=mesh['sp'=8,'tp'=4] {'tp'}, use_global_device_ids=true, to_apply=%region_10.11 | all-reduce | flops 256 | bytes 2048 | tf_op jit(solution)/shard_map/psum | solution.py:141
  215.2 1.3 collective-permute-start
  216.5 4.3 %fusion = bf16[1,2048,512]{2,1,0:T(8,128)(2,1)} fusion(bf16[512,2048]{1,0:T(8,128)(2,1)} %bitcast.121, bf16[512,512]{1,0:T(8,128)(2,1)S(1)} %copy-done.5), kind=kOutput, calls=%fused_computation.34 | convolution fusion | flops 1074790400 | bytes 4718592 | tf_op jit(solution)/shard_map/dot_general | solution.py:96
  221.9 2.0 fusion.32
  223.9 40.9 %reduce-scatter.2.cloned.1.call-done = bf16[256,512]{1,0:T(8,128)(2,1)} async-done(((bf16[2048,512]{1,0:T(8,128)(2,1)}), bf16[256,512]{1,0:T(8,128)(2,1)}) %reduce-scatter.2.cloned.1.call-update) | async-done | bytes 262160 | tf_op jit(solution)/shard_map/reduce_scatter | solution.py:124
  264.8 1.8 convert_element_type.72
  (126 shorter events, 8.1 us)
Async XLA Ops:
  7.2 48.3 %copy-start = (bf16[1,2048,512]{2,1,0:T(8,128)(2,1)S(1)}, bf16[1,2048,512]{2,1,0:T(8,128)(2,1)}, u32[]{:S(2)}) copy-start(bf16[1,2048,512]{2,1,0:T(8,128)(2,1)} %param.21) | copy-start | bytes 6291460
  7.2 26.5 %copy-start.39 = (f32[128,2]{0,1:T(2,128)S(1)}, f32[128,2]{0,1:T(2,128)}, u32[]{:S(2)}) copy-start(f32[128,2]{0,1:T(2,128)} %param.15) | copy-start | bytes 3076
  7.2 26.7 %copy-start.3 = (bf16[128,2048]{1,0:T(8,128)(2,1)S(1)}, bf16[128,2048]{1,0:T(8,128)(2,1)}, u32[]{:S(2)}) copy-start(bf16[128,2048]{1,0:T(8,128)(2,1)} %param.12) | copy-start | bytes 1572868
  7.2 48.2 %all-gather.5.cloned.1.call-start = ((), (), s32[]{:S(2)}) async-start(), calls=%async_computation.5 | async-start | bytes 2621440 | tf_op jit(solution)/shard_map/all_gather | solution.py:68
  33.7 45.9 %all-gather.3.cloned.1.call-start = ((), (), s32[]{:S(2)}) async-start(), calls=%async_computation.4 | async-start | bytes 2621440 | tf_op jit(solution)/shard_map/all_gather | solution.py:69
  51.9 88.2 %all-reduce.3.cloned.1.call-start = ((), (), s32[]{:S(2)}) async-start(), calls=%async_computation.6 | async-start | bytes 4194304 | tf_op jit(solution)/shard_map/psum | solution.py:105
  140.1 53.6 %all-to-all-start.2 = ((bf16[8,64,2048]{2,1,0:T(8,128)(2,1)}), bf16[8,64,2048]{2,1,0:T(8,128)(2,1)}, u32[]{:S(2)}, u32[]{:S(2)}) async-start(bf16[8,64,2048]{2,1,0:T(8,128)(2,1)} %all-reduce.3.cloned.1.call-done), calls=%async_computation.2 | async-start | bytes 4194304 | tf_op jit(solution)/shard_map/all_to_all | solution.py:106
  145.6 50.2 %copy-start.8 = (bf16[128,512]{1,0:T(8,128)(2,1)S(1)}, bf16[128,512]{1,0:T(8,128)(2,1)}, u32[]{:S(2)}) copy-start(bf16[128,512]{1,0:T(8,128)(2,1)} %param.16) | copy-start | bytes 393220
  145.6 50.2 %copy-start.37 = (f32[512]{0:T(512)S(1)}, f32[512]{0:T(512)}, u32[]{:S(2)}) copy-start(f32[512]{0:T(512)} %param.18) | copy-start | bytes 6148
  145.6 119.1 %reduce-scatter.2.cloned.1.call-start = ((), (), s32[]{:S(2)}) async-start(), calls=%async_computation.7 | async-start | bytes 2359296 | tf_op jit(solution)/shard_map/reduce_scatter | solution.py:124
  206.4 10.0 %copy-start.5 = (bf16[512,512]{1,0:T(8,128)(2,1)S(1)}, bf16[512,512]{1,0:T(8,128)(2,1)}, u32[]{:S(2)}) copy-start(bf16[512,512]{1,0:T(8,128)(2,1)} %copy-done.4) | copy-start | bytes 1572868
  214.9 6.8 %copy-start.10 = (f32[1,512]{1,0:T(1,128)S(1)}, f32[1,512]{1,0:T(1,128)}, u32[]{:S(2)}) copy-start(f32[1,512]{1,0:T(1,128)} %get-tuple-element.34) | copy-start | bytes 6148
  214.9 6.8 %copy-start.11 = (f32[1,512]{1,0:T(1,128)S(1)}, f32[1,512]{1,0:T(1,128)}, u32[]{:S(2)}) copy-start(f32[1,512]{1,0:T(1,128)} %get-tuple-element.35) | copy-start | bytes 6148
  214.9 6.8 %copy-start.12 = (f32[1,512]{1,0:T(1,128)S(1)}, f32[1,512]{1,0:T(1,128)}, u32[]{:S(2)}) copy-start(f32[1,512]{1,0:T(1,128)} %get-tuple-element.36) | copy-start | bytes 6148
  214.9 6.8 %copy-start.13 = (f32[1,512]{1,0:T(1,128)S(1)}, f32[1,512]{1,0:T(1,128)}, u32[]{:S(2)}) copy-start(f32[1,512]{1,0:T(1,128)} %get-tuple-element.37) | copy-start | bytes 6148
  214.9 6.8 %copy-start.14 = (f32[1,512]{1,0:T(1,128)S(1)}, f32[1,512]{1,0:T(1,128)}, u32[]{:S(2)}) copy-start(f32[1,512]{1,0:T(1,128)} %get-tuple-element.38) | copy-start | bytes 6148
  214.9 6.8 %copy-start.15 = (f32[1,512]{1,0:T(1,128)S(1)}, f32[1,512]{1,0:T(1,128)}, u32[]{:S(2)}) copy-start(f32[1,512]{1,0:T(1,128)} %get-tuple-element.39) | copy-start | bytes 6148
  214.9 6.8 %copy-start.16 = (f32[1,512]{1,0:T(1,128)S(1)}, f32[1,512]{1,0:T(1,128)}, u32[]{:S(2)}) copy-start(f32[1,512]{1,0:T(1,128)} %get-tuple-element.40) | copy-start | bytes 6148
  215.0 6.8 %copy-start.17 = (f32[1,512]{1,0:T(1,128)S(1)}, f32[1,512]{1,0:T(1,128)}, u32[]{:S(2)}) copy-start(f32[1,512]{1,0:T(1,128)} %get-tuple-element.41) | copy-start | bytes 6148
  215.0 6.8 %copy-start.18 = (f32[1,512]{1,0:T(1,128)S(1)}, f32[1,512]{1,0:T(1,128)}, u32[]{:S(2)}) copy-start(f32[1,512]{1,0:T(1,128)} %get-tuple-element.11) | copy-start | bytes 6148
  215.0 6.8 %copy-start.19 = (f32[1,512]{1,0:T(1,128)S(1)}, f32[1,512]{1,0:T(1,128)}, u32[]{:S(2)}) copy-start(f32[1,512]{1,0:T(1,128)} %get-tuple-element.12) | copy-start | bytes 6148
  215.0 6.8 %copy-start.20 = (f32[1,512]{1,0:T(1,128)S(1)}, f32[1,512]{1,0:T(1,128)}, u32[]{:S(2)}) copy-start(f32[1,512]{1,0:T(1,128)} %get-tuple-element.13) | copy-start | bytes 6148
  215.0 6.8 %copy-start.21 = (f32[1,512]{1,0:T(1,128)S(1)}, f32[1,512]{1,0:T(1,128)}, u32[]{:S(2)}) copy-start(f32[1,512]{1,0:T(1,128)} %get-tuple-element.14) | copy-start | bytes 6148
  215.2 6.5 %collective-permute-start = (f32[30,512]{1,0:T(8,128)S(1)}, f32[30,512]{1,0:T(8,128)S(1)}, u32[]{:S(2)}, u32[]{:S(2)}) collective-permute-start(f32[30,512]{1,0:T(8,128)S(1)} %slice.257), channel_id=1, source_target_pairs={{4,0},{8,4},{12,8},{16,12},{20,16},{24,20},{28,24},{5,1},{9,5},{13... | collective-permute-start | bytes 184328 | tf_op jit(solution)/shard_map/ppermute | solution.py:10
  (27 other events, 138.3 us)
Sparse Core Ops, SparseCore 0:
  33.8 21.5 all-gather.4
  57.0 22.5 all-gather.2
  88.7 51.3 all-reduce.2
  198.1 66.5 reduce-scatter.1
where the time goes:
time: 274 us; the launch traced here: 273 us
  waiting for transfers between devices  163 us (59%)
  blocking collectives  45.5 us (17%)
  matrix products  33.1 us (12%)
  between operations  14.5 us (5%)
  starting transfers between devices  6.96 us (3%)
  other arithmetic  6.52 us (2%)
  local copies, waits for them, and re-layouts  3.94 us (1%)
    psum x1, waiting for transfers between devices, shards(): summed = lax.psum(partial_value.astype(jnp.bfloat16), 'tp')  51.5 us
    all_to_all x1, waiting for transfers between devices, shards(): lax.all_to_all(summed.reshape(experts, capacity, model_width), 'sp', spli...  47.7 us
    reduce_scatter x1, waiting for transfers between devices, shards(): lax.psum_scatter(lax.dot_general(mixer_grad, act_conv, contract_first, pr...  40.9 us
    all_to_all x1, blocking collectives, shards(): lax.all_to_all(sent_rows, 'sp', split_axis=0, concat_axis=0, tiled=True)  21.7 us
    all_gather x1, waiting for transfers between devices, shards(): lax.all_gather(shared_rows[1], 'tp', axis=1, tiled=True)  17.9 us
    all_to_all x1, blocking collectives, shards(): lax.all_to_all(sent_grad, 'sp', split_axis=0, concat_axis=0, tiled=True)  17.6 us
    psum x1, blocking collectives, shards(): lax.psum((jnp.sum(norm_output_gradient, axis=1), jnp.sum(norm_output_grad...  6.16 us
    all_to_all x1, starting transfers between devices, shards(): lax.all_to_all(summed.reshape(experts, capacity, model_width), 'sp', spli...  5.51 us
  transfers between devices with their start and end apart: 6, of which 6 were waited for; matrix products, arithmetic and copies ran while one was open for 9% of the time, Pallas kernels for 0%

commit v1 on v0

--- a/solution.py
+++ b/solution.py
@@ -102,7 +102,7 @@
     partial_value = lax.dot_general(
         grad_gpre, w_first, contract_last, preferred_element_type=jnp.float32
     ) + lax.dot_general(grad_upre, w_third, contract_last, preferred_element_type=jnp.float32)
-    summed = lax.psum(partial_value.astype(jnp.bfloat16), "tp")
+    summed = jnp.sum(lax.all_gather(partial_value.astype(jnp.bfloat16), "tp"), axis=0)
     home_rows = lax.all_to_all(
         summed.reshape(experts, capacity, model_width),
         "sp",

time: 274 us -> 289 us (1.055)
  other arithmetic: 6.52 us -> 13.7 us
  waiting for transfers between devices: 163 us -> 170 us
    all_gather x0 -> x1, waiting for transfers between devices: none -> 58.4 us  [shards(): lax.all_gather(partial_value.astype(jnp.bfloat16), 'tp')]
    psum x1 -> x0, waiting for transfers between devices: 51.5 us -> none  [shards(): summed = lax.psum(partial_value.astype(jnp.bfloat16), 'tp')]
    reduce_sum x0 -> x1, other arithmetic: none -> 7.2 us  [shards(): jnp.sum(lax.all_gather(partial_value.astype(jnp.bfloat16), 'tp'), axis=0)]
  transfers between devices with their start and end apart: 6 -> 6, of which waited for: 6 -> 6; matrix products, arithmetic and copies ran while one was open for 9% -> 8% of each run, Pallas kernels for 0% -> 0%
where the time goes in v1:
time: 289 us; the launch traced here: 288 us
  waiting for transfers between devices  170 us (59%)
  blocking collectives  45.5 us (16%)
  matrix products  33.1 us (11%)
  between operations  14.5 us (5%)
  other arithmetic  13.7 us (5%)
  starting transfers between devices  7.15 us (2%)
  local copies, waits for them, and re-layouts  3.93 us (1%)
    all_gather x1, waiting for transfers between devices, shards(): lax.all_gather(partial_value.astype(jnp.bfloat16), 'tp')  58.4 us
    all_to_all x1, waiting for transfers between devices, shards(): lax.all_to_all(summed.reshape(experts, capacity, model_width), 'sp', spli...  48.2 us
    reduce_scatter x1, waiting for transfers between devices, shards(): lax.psum_scatter(lax.dot_general(mixer_grad, act_conv, contract_first, pr...  41.3 us
    all_to_all x1, blocking collectives, shards(): lax.all_to_all(sent_rows, 'sp', split_axis=0, concat_axis=0, tiled=True)  21.7 us
    all_gather x1, waiting for transfers between devices, shards(): lax.all_gather(shared_rows[1], 'tp', axis=1, tiled=True)  17.9 us
    all_to_all x1, blocking collectives, shards(): lax.all_to_all(sent_grad, 'sp', split_axis=0, concat_axis=0, tiled=True)  17.6 us
    reduce_sum x1, other arithmetic, shards(): jnp.sum(lax.all_gather(partial_value.astype(jnp.bfloat16), 'tp'), axis=0)  7.2 us
    psum x1, blocking collectives, shards(): lax.psum((jnp.sum(norm_output_gradient, axis=1), jnp.sum(norm_output_grad...  6.18 us
  transfers between devices with their start and end apart: 6, of which 6 were waited for; matrix products, arithmetic and copies ran while one was open for 8% of the time, Pallas kernels for 0%

profile of v1, /device:TPU:0, one launch (start us, length us, event | category | flops | bytes accessed | tf_op | source)
XLA Modules:
  0.0 288.0 jit_solution(13804271145828696299)
XLA Ops:
  10.6 1.3 convolution_convert_fusion.4
  11.9 21.7 %all_to_all.15 = bf16[8,16,2048]{2,1,0:T(8,128)(2,1)} all-to-all(bf16[8,16,2048]{2,1,0:T(8,128)(2,1)S(1)} %bitcast.89), channel_id=1, replica_groups=mesh['sp'=8,'tp'=4] {'sp'}, dimensions={0} | all-to-all | bytes 1048576 | tf_op jit(solution)/shard_map/all_to_all | solution.py:64
  34.2 17.6 %all_to_all.16 = bf16[8,16,2048]{2,1,0:T(8,128)(2,1)} all-to-all(bf16[8,16,2048]{2,1,0:T(8,128)(2,1)S(1)} %bitcast.88), channel_id=1, replica_groups=mesh['sp'=8,'tp'=4] {'sp'}, dimensions={0} | all-to-all | bytes 1048576 | tf_op jit(solution)/shard_map/all_to_all | solution.py:65
  51.9 3.5 %all-gather.7.cloned.1.call-done = bf16[8,64,2048]{2,1,0:T(8,128)(2,1)} async-done(((bf16[8,16,2048]{2,1,0:T(8,128)(2,1)}), bf16[8,64,2048]{2,1,0:T(8,128)(2,1)}) %all-gather.7.cloned.1.call-update) | async-done | bytes 2097168 | tf_op jit(solution)/shard_map/all_gather | solution.py:68
  55.4 4.0 %fusion.7 = f32[512,512]{1,0:T(8,128)} fusion(bf16[512,2048]{1,0:T(8,128)(2,1)} %bitcast.121, bf16[1,2048,512]{2,1,0:T(8,128)(2,1)S(1)} %copy-done), kind=kOutput, calls=%fused_computation.44 | convolution fusion | flops 1073741824 | bytes 5242880 | tf_op jit(solution)/shard_map/dot_general | solution.py:81
  59.4 2.3 fusion.10
  61.7 17.9 %all-gather.5.cloned.1.call-done = bf16[8,64,2048]{2,1,0:T(8,128)(2,1)} async-done(((bf16[8,16,2048]{2,1,0:T(8,128)(2,1)}), bf16[8,64,2048]{2,1,0:T(8,128)(2,1)}) %all-gather.5.cloned.1.call-update) | async-done | bytes 2097168 | tf_op jit(solution)/shard_map/all_gather | solution.py:69
  79.6 4.4 %multiply_convert_fusion.1 = (bf16[512,512]{1,0:T(8,128)(2,1)S(1)}, bf16[512,512]{1,0:T(8,128)(2,1)S(1)}) fusion(f32[512,512]{1,0:T(8,128)} %fusion.7, f32[512,512]{1,0:T(8,128)} %fusion.10, bf16[512,2048]{1,0:T(8,128)(2,1)} %bitcast.125, bf16[1,512,2048]{2,1,0:T(8,128)(2,1)} %param.23), kind=kOutput, calls=%fused_computation.55 | convolution fusion | flops 1077149696 | bytes 7340032 | tf_op jit(solution)/shard_map/dot_general | solution.py:89
  84.0 1.3 fusion.5
  85.9 2.6 add_convert_fusion
  88.6 58.4 %all-gather.9.cloned.1.call-done = bf16[2048,2048]{1,0:T(8,128)(2,1)} async-done(((bf16[512,2048]{1,0:T(8,128)(2,1)}), bf16[2048,2048]{1,0:T(8,128)(2,1)}) %all-gather.9.cloned.1.call-update) | async-done | bytes 8388624 | tf_op jit(solution)/shard_map/all_gather | solution.py:105
  147.0 7.2 %reduce_sum.54 = bf16[512,2048]{1,0:T(8,128)(2,1)} reduce(bf16[4,512,2048]{2,1,0:T(8,128)(2,1)} %bitcast.86, bf16[]{:T(256)} %constant.27.clone.1), dimensions={0}, to_apply=%region_6.7 | reduce | flops 3145728 | bytes 10485762 | tf_op jit(solution)/shard_map/reduce_sum | solution.py:105
  154.2 5.5 %all-to-all-start.2 = ((bf16[8,64,2048]{2,1,0:T(8,128)(2,1)}), bf16[8,64,2048]{2,1,0:T(8,128)(2,1)}, u32[]{:S(2)}, u32[]{:S(2)}) async-start(bf16[8,64,2048]{2,1,0:T(8,128)(2,1)} %bitcast.87), calls=%async_computation.2 | async-start | bytes 4194304 | tf_op jit(solution)/shard_map/all_to_all | solution.py:106
  160.3 48.2 %all-to-all-done.2 = bf16[8,64,2048]{2,1,0:T(8,128)(2,1)} async-done(((bf16[8,64,2048]{2,1,0:T(8,128)(2,1)}), bf16[8,64,2048]{2,1,0:T(8,128)(2,1)}, u32[]{:S(2)}, u32[]{:S(2)}) %all-to-all-start.2) | async-done | bytes 2097184 | tf_op jit(solution)/shard_map/all_to_all | solution.py:106
  208.5 2.1 fusion.4
  210.6 2.1 convolution_convert_fusion
  214.1 4.4 %fusion.1 = bf16[1,2048,512]{2,1,0:T(8,128)(2,1)} fusion(bf16[512,2048]{1,0:T(8,128)(2,1)} %bitcast.122, bf16[512,512]{1,0:T(8,128)(2,1)S(1)} %copy-done.7), kind=kOutput, calls=%fused_computation.35 | convolution fusion | flops 1074790400 | bytes 4718592 | tf_op jit(solution)/shard_map/dot_general | solution.py:99
  218.5 2.7 fusion.2
  221.2 1.5 fusion.128
  222.7 6.2 %all-reduce = (f32[128]{0:T(128)S(1)}, f32[128]{0:T(128)S(1)}) all-reduce(f32[128]{0:T(128)} %get-tuple-element.6, f32[128]{0:T(128)} %get-tuple-element.5), channel_id=1, replica_groups=mesh['sp'=8,'tp'=4] {'tp'}, use_global_device_ids=true, to_apply=%region_10.11 | all-reduce | flops 256 | bytes 2048 | tf_op jit(solution)/shard_map/psum | solution.py:141
  231.2 4.3 %fusion = bf16[1,2048,512]{2,1,0:T(8,128)(2,1)} fusion(bf16[512,2048]{1,0:T(8,128)(2,1)} %bitcast.123, bf16[512,512]{1,0:T(8,128)(2,1)S(1)} %copy-done.5), kind=kOutput, calls=%fused_computation.34 | convolution fusion | flops 1074790400 | bytes 4718592 | tf_op jit(solution)/shard_map/dot_general | solution.py:96
  236.4 2.0 fusion.32
  238.4 41.3 %reduce-scatter.2.cloned.1.call-done = bf16[256,512]{1,0:T(8,128)(2,1)} async-done(((bf16[2048,512]{1,0:T(8,128)(2,1)}), bf16[256,512]{1,0:T(8,128)(2,1)}) %reduce-scatter.2.cloned.1.call-update) | async-done | bytes 262160 | tf_op jit(solution)/shard_map/reduce_scatter | solution.py:124
  279.7 1.8 convert_element_type.74
  (127 shorter events, 9.3 us)
Async XLA Ops:
  7.2 48.3 %copy-start = (bf16[1,2048,512]{2,1,0:T(8,128)(2,1)S(1)}, bf16[1,2048,512]{2,1,0:T(8,128)(2,1)}, u32[]{:S(2)}) copy-start(bf16[1,2048,512]{2,1,0:T(8,128)(2,1)} %param.21) | copy-start | bytes 6291460
  7.2 26.5 %copy-start.39 = (f32[128,2]{0,1:T(2,128)S(1)}, f32[128,2]{0,1:T(2,128)}, u32[]{:S(2)}) copy-start(f32[128,2]{0,1:T(2,128)} %param.15) | copy-start | bytes 3076
  7.2 26.7 %copy-start.3 = (bf16[128,2048]{1,0:T(8,128)(2,1)S(1)}, bf16[128,2048]{1,0:T(8,128)(2,1)}, u32[]{:S(2)}) copy-start(bf16[128,2048]{1,0:T(8,128)(2,1)} %param.12) | copy-start | bytes 1572868
  7.2 48.2 %all-gather.7.cloned.1.call-start = ((), (), s32[]{:S(2)}) async-start(), calls=%async_computation.5 | async-start | bytes 2621440 | tf_op jit(solution)/shard_map/all_gather | solution.py:68
  33.7 45.9 %all-gather.5.cloned.1.call-start = ((), (), s32[]{:S(2)}) async-start(), calls=%async_computation.4 | async-start | bytes 2621440 | tf_op jit(solution)/shard_map/all_gather | solution.py:69
  51.9 95.1 %all-gather.9.cloned.1.call-start = ((), (), s32[]{:S(2)}) async-start(), calls=%async_computation.7 | async-start | bytes 10485760 | tf_op jit(solution)/shard_map/all_gather | solution.py:105
  154.2 54.3 %all-to-all-start.2 = ((bf16[8,64,2048]{2,1,0:T(8,128)(2,1)}), bf16[8,64,2048]{2,1,0:T(8,128)(2,1)}, u32[]{:S(2)}, u32[]{:S(2)}) async-start(bf16[8,64,2048]{2,1,0:T(8,128)(2,1)} %bitcast.87), calls=%async_computation.2 | async-start | bytes 4194304 | tf_op jit(solution)/shard_map/all_to_all | solution.py:106
  159.7 50.8 %copy-start.8 = (bf16[128,512]{1,0:T(8,128)(2,1)S(1)}, bf16[128,512]{1,0:T(8,128)(2,1)}, u32[]{:S(2)}) copy-start(bf16[128,512]{1,0:T(8,128)(2,1)} %param.16) | copy-start | bytes 393220
  159.7 50.8 %copy-start.37 = (f32[512]{0:T(512)S(1)}, f32[512]{0:T(512)}, u32[]{:S(2)}) copy-start(f32[512]{0:T(512)} %param.18) | copy-start | bytes 6148
  159.7 120.0 %reduce-scatter.2.cloned.1.call-start = ((), (), s32[]{:S(2)}) async-start(), calls=%async_computation.6 | async-start | bytes 2359296 | tf_op jit(solution)/shard_map/reduce_scatter | solution.py:124
  221.2 10.1 %copy-start.5 = (bf16[512,512]{1,0:T(8,128)(2,1)S(1)}, bf16[512,512]{1,0:T(8,128)(2,1)}, u32[]{:S(2)}) copy-start(bf16[512,512]{1,0:T(8,128)(2,1)} %copy-done.4) | copy-start | bytes 1572868
  229.7 6.5 %copy-start.10 = (f32[1,512]{1,0:T(1,128)S(1)}, f32[1,512]{1,0:T(1,128)}, u32[]{:S(2)}) copy-start(f32[1,512]{1,0:T(1,128)} %get-tuple-element.34) | copy-start | bytes 6148
  229.7 6.5 %copy-start.11 = (f32[1,512]{1,0:T(1,128)S(1)}, f32[1,512]{1,0:T(1,128)}, u32[]{:S(2)}) copy-start(f32[1,512]{1,0:T(1,128)} %get-tuple-element.35) | copy-start | bytes 6148
  229.7 6.5 %copy-start.12 = (f32[1,512]{1,0:T(1,128)S(1)}, f32[1,512]{1,0:T(1,128)}, u32[]{:S(2)}) copy-start(f32[1,512]{1,0:T(1,128)} %get-tuple-element.36) | copy-start | bytes 6148
  229.7 6.5 %copy-start.13 = (f32[1,512]{1,0:T(1,128)S(1)}, f32[1,512]{1,0:T(1,128)}, u32[]{:S(2)}) copy-start(f32[1,512]{1,0:T(1,128)} %get-tuple-element.37) | copy-start | bytes 6148
  229.7 6.5 %copy-start.14 = (f32[1,512]{1,0:T(1,128)S(1)}, f32[1,512]{1,0:T(1,128)}, u32[]{:S(2)}) copy-start(f32[1,512]{1,0:T(1,128)} %get-tuple-element.38) | copy-start | bytes 6148
  229.7 6.5 %copy-start.15 = (f32[1,512]{1,0:T(1,128)S(1)}, f32[1,512]{1,0:T(1,128)}, u32[]{:S(2)}) copy-start(f32[1,512]{1,0:T(1,128)} %get-tuple-element.39) | copy-start | bytes 6148
  229.7 6.5 %copy-start.16 = (f32[1,512]{1,0:T(1,128)S(1)}, f32[1,512]{1,0:T(1,128)}, u32[]{:S(2)}) copy-start(f32[1,512]{1,0:T(1,128)} %get-tuple-element.40) | copy-start | bytes 6148
  229.7 6.5 %copy-start.17 = (f32[1,512]{1,0:T(1,128)S(1)}, f32[1,512]{1,0:T(1,128)}, u32[]{:S(2)}) copy-start(f32[1,512]{1,0:T(1,128)} %get-tuple-element.41) | copy-start | bytes 6148
  229.7 6.5 %copy-start.18 = (f32[1,512]{1,0:T(1,128)S(1)}, f32[1,512]{1,0:T(1,128)}, u32[]{:S(2)}) copy-start(f32[1,512]{1,0:T(1,128)} %get-tuple-element.11) | copy-start | bytes 6148
  229.8 6.5 %copy-start.19 = (f32[1,512]{1,0:T(1,128)S(1)}, f32[1,512]{1,0:T(1,128)}, u32[]{:S(2)}) copy-start(f32[1,512]{1,0:T(1,128)} %get-tuple-element.12) | copy-start | bytes 6148
  229.8 6.5 %copy-start.20 = (f32[1,512]{1,0:T(1,128)S(1)}, f32[1,512]{1,0:T(1,128)}, u32[]{:S(2)}) copy-start(f32[1,512]{1,0:T(1,128)} %get-tuple-element.13) | copy-start | bytes 6148
  229.8 6.5 %copy-start.21 = (f32[1,512]{1,0:T(1,128)S(1)}, f32[1,512]{1,0:T(1,128)}, u32[]{:S(2)}) copy-start(f32[1,512]{1,0:T(1,128)} %get-tuple-element.14) | copy-start | bytes 6148
  229.9 6.2 %collective-permute-start = (f32[30,512]{1,0:T(8,128)S(1)}, f32[30,512]{1,0:T(8,128)S(1)}, u32[]{:S(2)}, u32[]{:S(2)}) collective-permute-start(f32[30,512]{1,0:T(8,128)S(1)} %slice.257), channel_id=1, source_target_pairs={{4,0},{8,4},{12,8},{16,12},{20,16},{24,20},{28,24},{5,1},{9,5},{13... | collective-permute-start | bytes 184328 | tf_op jit(solution)/shard_map/ppermute | solution.py:10
  (27 other events, 134.3 us)
Sparse Core Ops, SparseCore 0:
  33.8 21.5 all-gather.6
  57.0 22.5 all-gather.4
  88.7 58.2 all-gather.8
  212.8 66.7 reduce-scatter.1
